TPU v7x, 256 devices: a whole 4x4x8 slice. The times are simulated.
256 devices in a mesh: kv: 16 (over y, x), tp: 16 (over z, core).
Axes of the slice: x: 4, y: 4, z: 8, core: 2. Of those that a mesh axis runs over, the one named last changes fastest.
Arguments:
- tokens: bfloat16 [256, 4096], P('kv', 'tp'), may hold values from -6 to 6
- attn_gain: float32 [4096], replicated, may hold values from 0.1 to 1.9
- w_query: bfloat16 [4096, 2048], P(None, 'tp'), may hold values from -0.09375 to 0.09375
- w_key: bfloat16 [4096, 2048], P(None, 'tp'), may hold values from -0.09375 to 0.09375
- w_value: bfloat16 [4096, 2048], P(None, 'tp'), may hold values from -0.09375 to 0.09375
- w_outgate: bfloat16 [4096, 2048], P(None, 'tp'), may hold values from -0.09375 to 0.09375
- w_rates: bfloat16 [2, 4096, 16], P(None, None, 'tp'), may hold values from -0.09375 to 0.09375
- head_rate: float32 [16], P('tp'), may hold values from 0.02 to 2
- head_gain: float32 [2048], P('tp'), may hold values from 0.1 to 1.9
- w_out: bfloat16 [2048, 4096], P('tp'), may hold values from -0.125 to 0.125
- state: float32 [256, 16, 128, 128], P('kv', 'tp'), may hold values from -2.4 to 2.4
- mlp_gain: float32 [4096], replicated, may hold values from 0.1 to 1.9
- w_gate: bfloat16 [4096, 11264], P(None, ('kv', 'tp')), may hold values from -0.09375 to 0.09375
- w_up: bfloat16 [4096, 11264], P(None, ('kv', 'tp')), may hold values from -0.09375 to 0.09375
- w_down: bfloat16 [4096, 11264], P(None, ('kv', 'tp')), may hold values from -0.25 to 0.25
Outputs:
- result: bfloat16 [256, 4096], P('kv', 'tp')
- new_state: float32 [256, 16, 128, 128], P('kv', 'tp')
All inputs are finite; a program needn't handle non-finite values.
Results may differ from a plain program's by a relative error of at most 0.014.
Values may be sent and summed in bfloat16 or wider, within the bound.
No kernel may reach another device: no remote copies, remote signals or barrier semaphores. Data moves between devices by JAX's collectives and lax.ppermute only.
A program may use at most 64 MiB of HBM per device.

v0:
```python
import jax
import jax.numpy as jnp
from jax import lax
from jax.sharding import PartitionSpec as P

EPS = 1e-06


def copy_for_each(value, axis):
    size = lax.axis_size(axis)
    return lax.all_to_all(
        jnp.broadcast_to(value[None], (size, *value.shape)), axis, 0, 0, tiled=True
    )


def in_order(tiles, dim):
    lengths = list(tiles.shape[1:])
    lengths[dim] *= tiles.shape[0]
    return jnp.moveaxis(tiles, 0, dim).reshape(lengths)


def gather_directly(value, axis, dim):
    tiles = copy_for_each(value, axis)
    return in_order(tiles, dim)


def cut_along(value, dim, size):
    lengths = value.shape
    tiles = value.reshape(*lengths[:dim], size, lengths[dim] // size, *lengths[dim + 1 :])
    return jnp.moveaxis(tiles, dim, 0)


def sent_and_summed(value, axis, dim):
    size = lax.axis_size(axis)
    tiles = lax.all_to_all(cut_along(value, dim, size), axis, 0, 0, tiled=True)
    return jnp.sum(tiles.astype(jnp.float32), axis=0)


def sent_and_summed_2(value, axis, dim):
    tiles = cut_along(value, dim, lax.axis_size(axis))
    arrived = lax.all_to_all(tiles, axis, split_axis=0, concat_axis=0, tiled=True)
    return arrived.sum(axis=0)


def row_norm(values, gain):
    floats = values.astype(jnp.float32)
    scaled = floats * lax.rsqrt(jnp.mean(floats * floats, axis=-1, keepdims=True) + EPS)
    return (scaled * gain).astype(jnp.bfloat16)


def hidden_units(normed_mlp, gate_part, up_part):
    gate_pre = jnp.dot(normed_mlp, gate_part, preferred_element_type=jnp.float32)
    up_pre = jnp.dot(normed_mlp, up_part, preferred_element_type=jnp.float32)
    return (jax.nn.silu(gate_pre) * up_pre).astype(jnp.bfloat16)


def down_product(hidden, down_part):
    return lax.dot_general(
        hidden, down_part, (((1,), (1,)), ((), ())), preferred_element_type=jnp.float32
    )


def body(
    tokens,
    attn_gain,
    w_query,
    w_key,
    w_value,
    w_outgate,
    w_rates,
    head_rate,
    head_gain,
    w_out,
    state,
    mlp_gain,
    w_gate,
    w_up,
    w_down,
):
    count = tokens.shape[0]
    local_heads = head_rate.shape[0]
    size = w_query.shape[1] // local_heads
    whole_rows = gather_directly(tokens, "tp", 1)
    normed = row_norm(whole_rows, attn_gain)
    query = jnp.dot(normed, w_query, preferred_element_type=jnp.float32).reshape(
        count, local_heads, size
    )
    key = jnp.dot(normed, w_key, preferred_element_type=jnp.float32).reshape(
        count, local_heads, size
    )
    value = jnp.dot(normed, w_value, preferred_element_type=jnp.float32).reshape(
        count, local_heads, size
    )
    gate_in = jnp.dot(normed, w_outgate, preferred_element_type=jnp.float32).reshape(
        count, local_heads, size
    )
    rates = jnp.einsum("bd,sdh->sbh", normed, w_rates, preferred_element_type=jnp.float32)
    unit_query = (
        query * lax.rsqrt(jnp.sum(query * query, axis=-1, keepdims=True) + EPS) * size ** (-0.5)
    )
    unit_key = key * lax.rsqrt(jnp.sum(key * key, axis=-1, keepdims=True) + EPS)
    strength = jax.nn.sigmoid(rates[0])
    fade = jnp.exp(-head_rate * jax.nn.softplus(rates[1]))
    carried = state * fade[:, :, None, None]
    fresh = strength[:, :, None] * (value - jnp.einsum("bhi,bhiv->bhv", unit_key, carried))
    new_state = carried + unit_key[:, :, :, None] * fresh[:, :, None, :]
    readout = jnp.einsum("bhi,bhiv->bhv", unit_query, new_state)
    normed_out = readout * lax.rsqrt(jnp.mean(readout * readout, axis=-1, keepdims=True) + EPS)
    mixed = (normed_out * head_gain.reshape(local_heads, size) * jax.nn.silu(gate_in)).astype(
        jnp.bfloat16
    )
    partial_value = jnp.dot(
        mixed.reshape(count, local_heads * size), w_out, preferred_element_type=jnp.float32
    )
    projected = sent_and_summed(partial_value.astype(jnp.bfloat16), "tp", 1)
    residual = (tokens.astype(jnp.float32) + projected).astype(jnp.bfloat16)
    full_residual = gather_directly(residual, "tp", 1)
    normed_mlp = row_norm(full_residual, mlp_gain)
    shared_rows = gather_directly(normed_mlp, "kv", 0)
    hidden = hidden_units(shared_rows, w_gate, w_up)
    owned = lax.all_to_all(hidden, "kv", split_axis=0, concat_axis=1, tiled=True)
    folded = down_product(owned, lax.all_gather(w_down, "kv", axis=1, tiled=True))
    down = sent_and_summed_2(folded, "tp", 1)
    result = (residual.astype(jnp.float32) + down).astype(jnp.bfloat16)
    return (result, new_state)


def solution(mesh):
    return jax.shard_map(
        body,
        mesh=mesh,
        in_specs=(
            P("kv", "tp"),
            P(),
            P(None, "tp"),
            P(None, "tp"),
            P(None, "tp"),
            P(None, "tp"),
            P(None, None, "tp"),
            P("tp"),
            P("tp"),
            P("tp", None),
            P("kv", "tp", None, None),
            P(),
            P(None, ("kv", "tp")),
            P(None, ("kv", "tp")),
            P(None, ("kv", "tp")),
        ),
        out_specs=(P("kv", "tp"), P("kv", "tp", None, None)),
        check_vma=False,
    )
```

profile of v0, /device:TPU:1, one launch (start us, length us, event | category | flops | bytes accessed | tf_op | source)
XLA Modules:
  0.0 156.5 jit_solution(1678312154421125208)
XLA Ops:
  7.2 0.7 all-gather.3.cloned.1.call-update
  7.9 1.4 broadcast_in_dim.6
  9.3 10.0 %all-to-all-start = ((bf16[16,16,256]{2,1,0:T(8,128)(2,1)}), bf16[16,16,256]{2,1,0:T(8,128)(2,1)S(1)}, u32[]{:S(2)}, u32[]{:S(2)}) async-start(bf16[16,16,256]{2,1,0:T(8,128)(2,1)} %broadcast_in_dim.6), calls=%async_computation | async-start | bytes 262144 | tf_op jit(solution)/shard_map/all_to_all | solution.py:11
  19.9 0.7 mul.205
  20.6 7.5 %all-to-all-done = bf16[16,16,256]{2,1,0:T(8,128)(2,1)S(1)} async-done(((bf16[16,16,256]{2,1,0:T(8,128)(2,1)}), bf16[16,16,256]{2,1,0:T(8,128)(2,1)S(1)}, u32[]{:S(2)}, u32[]{:S(2)}) %all-to-all-start) | async-done | bytes 131104 | tf_op jit(solution)/shard_map/all_to_all | solution.py:11
  28.6 0.4 multiply_reduce_fusion.1
  29.0 0.4 copy-done.3
  29.4 0.4 multiply_reduce_fusion.2
  30.1 0.3 fusion.10
  30.4 0.3 fusion.7
  30.7 0.5 fusion.33
  31.4 0.5 convolution_convert_fusion
  31.9 11.6 %all_to_all.44 = bf16[16,16,256]{2,1,0:T(8,128)(2,1)S(1)} all-to-all(bf16[16,16,256]{2,1,0:T(8,128)(2,1)S(1)} %bitcast.108), channel_id=1, replica_groups=mesh['kv'=16,'tp'=16] {'tp'}, dimensions={0} | all-to-all | bytes 262144 | tf_op jit(solution)/shard_map/all_to_all | solution.py:35
  43.5 11.6 %all_to_all.45 = bf16[16,16,256]{2,1,0:T(8,128)(2,1)S(1)} all-to-all(bf16[16,16,256]{2,1,0:T(8,128)(2,1)S(1)} %broadcast_in_dim.7), channel_id=1, replica_groups=mesh['kv'=16,'tp'=16] {'tp'}, dimensions={0} | all-to-all | bytes 262144 | tf_op jit(solution)/shard_map/all_to_all | solution.py:11
  55.6 49.6 %all_to_all.46 = bf16[16,16,4096]{2,1,0:T(8,128)(2,1)S(1)} all-to-all(bf16[16,16,4096]{2,1,0:T(8,128)(2,1)S(1)} %broadcast_in_dim.8), channel_id=1, replica_groups=mesh['kv'=16,'tp'=16] {'kv'}, dimensions={0} | all-to-all | bytes 4194304 | tf_op jit(solution)/shard_map/all_to_all | solution.py:11
  105.2 0.7 fusion.36
  106.2 0.7 fusion.6
  107.3 9.0 %all_to_all.47 = bf16[16,2,352]{2,1,0:T(2,128)(2,1)S(1)} all-to-all(bf16[16,2,352]{2,1,0:T(2,128)(2,1)S(1)} %reshape.265), channel_id=1, replica_groups=mesh['kv'=16,'tp'=16] {'kv'}, dimensions={0} | all-to-all | bytes 45056 | tf_op jit(solution)/shard_map/all_to_all | solution.py:121
  116.5 8.0 %reshape.258 = bf16[704,4096]{1,0:T(8,128)(2,1)} reshape(bf16[16,44,4096]{2,1,0:T(8,128)(2,1)} %all-gather.3.cloned.1.call-done) | data formatting | bytes 11534336
  124.6 4.2 %fusion.3 = f32[16,16,256]{2,1,0:T(8,128)} fusion(bf16[16,704,1]{1,0,2:T(8,128)(2,1)S(1)} %reshape.263, bf16[88,16,8,256]{3,2,1,0:T(8,128)(2,1)} %bitcast.102), kind=kOutput, calls=%fused_computation.4 | convolution fusion | flops 92274688 | bytes 6051840 | tf_op jit(solution)/shard_map/dot_general | solution.py:58
  128.8 8.7 %all-to-all-start.5 = ((f32[16,16,256]{2,1,0:T(8,128)}), f32[16,16,256]{2,1,0:T(8,128)S(1)}, u32[]{:S(2)}, u32[]{:S(2)}) async-start(f32[16,16,256]{2,1,0:T(8,128)} %fusion.3), calls=%async_computation.5 | async-start | bytes 524288 | tf_op jit(solution)/shard_map/all_to_all | solution.py:41
  137.5 1.3 multiply_add_fusion
  138.8 10.3 %all-to-all-done.5 = f32[16,16,256]{2,1,0:T(8,128)S(1)} async-done(((f32[16,16,256]{2,1,0:T(8,128)}), f32[16,16,256]{2,1,0:T(8,128)S(1)}, u32[]{:S(2)}, u32[]{:S(2)}) %all-to-all-start.5) | async-done | bytes 262176 | tf_op jit(solution)/shard_map/all_to_all | solution.py:41
  149.1 0.6 add_convert_fusion
  (59 shorter events, 2.4 us)
Async XLA Ops:
  7.2 24.2 %copy-start = (bf16[128,4096]{1,0:T(8,128)(2,1)S(1)}, bf16[128,4096]{1,0:T(8,128)(2,1)}, u32[]{:S(2)}) copy-start(bf16[128,4096]{1,0:T(8,128)(2,1)} %param.24) | copy-start | bytes 3145732
  7.2 21.3 %copy-start.8 = (f32[4096]{0:T(1024)S(1)}, f32[4096]{0:T(1024)}, u32[]{:S(2)}) copy-start(f32[4096]{0:T(1024)} %param.16) | copy-start | bytes 49156
  7.2 21.4 %copy-start.2 = (bf16[4096,128]{1,0:T(8,128)(2,1)S(1)}, bf16[4096,128]{1,0:T(8,128)(2,1)}, u32[]{:S(2)}) copy-start(bf16[4096,128]{1,0:T(8,128)(2,1)} %param.18) | copy-start | bytes 3145732
  7.2 109.3 %all-gather.3.cloned.1.call-start = ((), (), s32[]{:S(2)}) async-start(), calls=%async_computation.6 | async-start | bytes 6684672 | tf_op jit(solution)/shard_map/all_gather | solution.py:122
  9.3 18.9 %all-to-all-start = ((bf16[16,16,256]{2,1,0:T(8,128)(2,1)}), bf16[16,16,256]{2,1,0:T(8,128)(2,1)S(1)}, u32[]{:S(2)}, u32[]{:S(2)}) async-start(bf16[16,16,256]{2,1,0:T(8,128)(2,1)} %broadcast_in_dim.6), calls=%async_computation | async-start | bytes 262144 | tf_op jit(solution)/shard_map/all_to_all | solution.py:11
  28.2 1.2 copy-start.3
  28.3 1.4 copy-start.12
  28.4 1.7 %copy-start.1 = (f32[16,1,128,128]{3,2,1,0:T(8,128)S(1)}, f32[16,1,128,128]{3,2,1,0:T(8,128)}, u32[]{:S(2)}) copy-start(f32[16,1,128,128]{3,2,1,0:T(8,128)} %param.25) | copy-start | bytes 3145732
  28.5 1.9 %copy-start.4 = (bf16[4096,128]{1,0:T(8,128)(2,1)S(1)}, bf16[4096,128]{1,0:T(8,128)(2,1)}, u32[]{:S(2)}) copy-start(bf16[4096,128]{1,0:T(8,128)(2,1)} %param.19) | copy-start | bytes 3145732
  29.4 2.0 %copy-start.5 = (bf16[4096,128]{1,0:T(8,128)(2,1)S(1)}, bf16[4096,128]{1,0:T(8,128)(2,1)}, u32[]{:S(2)}) copy-start(bf16[4096,128]{1,0:T(8,128)(2,1)} %param.20) | copy-start | bytes 3145732
  29.4 2.0 %copy-start.11 = (f32[128]{0:T(128)S(1)}, f32[128]{0:T(128)}, u32[]{:S(2)}) copy-start(f32[128]{0:T(128)} %param.23) | copy-start | bytes 1540
  30.7 12.8 %copy-start.9 = (bf16[16,256]{1,0:T(8,128)(2,1)S(1)}, bf16[16,256]{1,0:T(8,128)(2,1)}, u32[]{:S(2)}) copy-start(bf16[16,256]{1,0:T(8,128)(2,1)} %param.15) | copy-start | bytes 24580
  31.4 23.9 %copy-start.10 = (f32[4096]{0:T(1024)S(1)}, f32[4096]{0:T(1024)}, u32[]{:S(2)}) copy-start(f32[4096]{0:T(1024)} %param.26) | copy-start | bytes 49156
  55.6 49.6 %copy-start.6 = (bf16[4096,44]{0,1:T(8,128)(2,1)S(1)}, bf16[4096,44]{0,1:T(8,128)(2,1)}, u32[]{:S(2)}) copy-start(bf16[4096,44]{0,1:T(8,128)(2,1)} %param.27) | copy-start | bytes 1081348
  105.2 1.0 copy-start.7
  128.8 20.3 %all-to-all-start.5 = ((f32[16,16,256]{2,1,0:T(8,128)}), f32[16,16,256]{2,1,0:T(8,128)S(1)}, u32[]{:S(2)}, u32[]{:S(2)}) async-start(f32[16,16,256]{2,1,0:T(8,128)} %fusion.3), calls=%async_computation.5 | async-start | bytes 524288 | tf_op jit(solution)/shard_map/all_to_all | solution.py:41
Sparse Core Ops, SparseCore 0:
  10.4 91.6 all-gather.2
where the time goes:
time: 157 us
  blocking collectives  81.7 us (52%)
  starting transfers between devices  18.7 us (12%)
  waiting for transfers between devices  18.5 us (12%)
  between operations  15 us (10%)
  local copies, waits for them, and re-layouts  11.6 us (7%)
  matrix products  8.08 us (5%)
  other arithmetic  2.96 us (2%)
    all_to_all x2, blocking collectives, copy_for_each(): lax.all_to_all(jnp.broadcast_to(value[None], (size, *value.shape)), axis,...  61.2 us
    all_to_all x1, blocking collectives, sent_and_summed(): tiles = lax.all_to_all(cut_along(value, dim, size), axis, 0, 0, tiled=True)  11.6 us
    all_to_all x1, waiting for transfers between devices, sent_and_summed_2(): lax.all_to_all(tiles, axis, split_axis=0, concat_axis=0, tiled=True)  10.3 us
    all_to_all x1, starting transfers between devices, copy_for_each(): lax.all_to_all(jnp.broadcast_to(value[None], (size, *value.shape)), axis,...  9.97 us
    all_to_all x1, blocking collectives, body(): lax.all_to_all(hidden, 'kv', split_axis=0, concat_axis=1, tiled=True)  8.99 us
    unnamed x29, local copies, waits for them, and re-layouts  8.94 us
    all_to_all x1, starting transfers between devices, sent_and_summed_2(): lax.all_to_all(tiles, axis, split_axis=0, concat_axis=0, tiled=True)  8.69 us
    all_to_all x1, waiting for transfers between devices, copy_for_each(): lax.all_to_all(jnp.broadcast_to(value[None], (size, *value.shape)), axis,...  7.51 us
  transfers between devices with their start and end apart: 3, of which 2 were waited for; matrix products, arithmetic and copies ran while one was open for 6% of the time, Pallas kernels for 0%

commit v1 on v0

--- a/solution.py
+++ b/solution.py
@@ -118,7 +118,19 @@
     normed_mlp = row_norm(full_residual, mlp_gain)
     shared_rows = gather_directly(normed_mlp, "kv", 0)
     hidden = hidden_units(shared_rows, w_gate, w_up)
-    owned = lax.all_to_all(hidden, "kv", split_axis=0, concat_axis=1, tiled=True)
+    ways, here = (lax.axis_size("kv"), lax.axis_index("kv"))
+    width = hidden.shape[0] // ways
+    lengths_2 = list(hidden.shape)
+    lengths_2[0] = width
+    height = lengths_2[1]
+    lengths_2[1] = height * ways
+    full = jnp.zeros(lengths_2, hidden.dtype)
+    for mask in range(ways):
+        part = lax.dynamic_slice_in_dim(hidden, (here ^ mask) * width, width, axis=0)
+        if mask:
+            part = lax.ppermute(part, "kv", [(d, d ^ mask) for d in range(ways)])
+        full = lax.dynamic_update_slice_in_dim(full, part, (here ^ mask) * height, axis=1)
+    owned = full
     folded = down_product(owned, lax.all_gather(w_down, "kv", axis=1, tiled=True))
     down = sent_and_summed_2(folded, "tp", 1)
     result = (residual.astype(jnp.float32) + down).astype(jnp.bfloat16)

time: 157 us -> 180 us (1.15)
  blocking collectives: 81.7 us -> 23.1 us
  waiting for transfers between devices: 18.5 us -> 61.7 us
  starting transfers between devices: 18.7 us -> 51.2 us
  local copies, waits for them, and re-layouts: 11.6 us -> 17.3 us
    all_to_all x2 -> x1, blocking collectives: 61.2 us -> 11.6 us  [copy_for_each(): lax.all_to_all(jnp.broadcast_to(value[None], (size, *value.shape)), axis,...]
    all_to_all x1 -> x2, waiting for transfers between devices: 7.51 us -> 50.7 us  [copy_for_each(): lax.all_to_all(jnp.broadcast_to(value[None], (size, *value.shape)), axis,...]
    ppermute x0 -> x15, starting transfers between devices: none -> 24.2 us  [body(): part = lax.ppermute(part, 'kv', [(d, d ^ mask) for d in range(ways)])]
    all_to_all x1 -> x0, blocking collectives: 8.99 us -> none  [body(): lax.all_to_all(hidden, 'kv', split_axis=0, concat_axis=1, tiled=True)]
    all_to_all x1 -> x2, starting transfers between devices: 9.97 us -> 16.9 us  [copy_for_each(): lax.all_to_all(jnp.broadcast_to(value[None], (size, *value.shape)), axis,...]
    dynamic_update_slice x0 -> x16, local copies, waits for them, and re-layouts: none -> 3.67 us  [body(): lax.dynamic_update_slice_in_dim(full, part, (here ^ mask) * height, axis=1)]
    unnamed x29 -> x37, local copies, waits for them, and re-layouts: 8.94 us -> 8.94 us
  transfers between devices with their start and end apart: 3 -> 19, of which waited for: 2 -> 3; matrix products, arithmetic and copies ran while one was open for 6% -> 8% of each run, Pallas kernels for 0% -> 0%
where the time goes in v1:
time: 180 us; the launch traced here: 179 us
  waiting for transfers between devices  61.7 us (34%)
  starting transfers between devices  51.2 us (28%)
  blocking collectives  23.1 us (13%)
  local copies, waits for them, and re-layouts  17.3 us (10%)
  between operations  15.4 us (9%)
  matrix products  7.48 us (4%)
  other arithmetic  2.96 us (2%)
    all_to_all x2, waiting for transfers between devices, copy_for_each(): lax.all_to_all(jnp.broadcast_to(value[None], (size, *value.shape)), axis,...  50.7 us
    ppermute x15, starting transfers between devices, body(): part = lax.ppermute(part, 'kv', [(d, d ^ mask) for d in range(ways)])  24.2 us
    all_to_all x2, starting transfers between devices, copy_for_each(): lax.all_to_all(jnp.broadcast_to(value[None], (size, *value.shape)), axis,...  16.9 us
    all_to_all x1, blocking collectives, sent_and_summed(): tiles = lax.all_to_all(cut_along(value, dim, size), axis, 0, 0, tiled=True)  11.6 us
    all_to_all x1, blocking collectives, copy_for_each(): lax.all_to_all(jnp.broadcast_to(value[None], (size, *value.shape)), axis,...  11.6 us
    all_to_all x1, waiting for transfers between devices, sent_and_summed_2(): lax.all_to_all(tiles, axis, split_axis=0, concat_axis=0, tiled=True)  10.2 us
    all_to_all x1, starting transfers between devices, sent_and_summed_2(): lax.all_to_all(tiles, axis, split_axis=0, concat_axis=0, tiled=True)  10.2 us
    unnamed x37, local copies, waits for them, and re-layouts  8.94 us
  transfers between devices with their start and end apart: 19, of which 3 were waited for; matrix products, arithmetic and copies ran while one was open for 8% of the time, Pallas kernels for 0%

profile of v1, /device:TPU:1, one launch (start us, length us, event | category | flops | bytes accessed | tf_op | source)
XLA Modules:
  0.0 179.2 jit_solution(17767848905073000115)
XLA Ops:
  7.9 1.4 broadcast_in_dim.8
  9.3 10.0 %all-to-all-start = ((bf16[16,16,256]{2,1,0:T(8,128)(2,1)}), bf16[16,16,256]{2,1,0:T(8,128)(2,1)S(1)}, u32[]{:S(2)}, u32[]{:S(2)}) async-start(bf16[16,16,256]{2,1,0:T(8,128)(2,1)} %broadcast_in_dim.8), calls=%async_computation | async-start | bytes 262144 | tf_op jit(solution)/shard_map/all_to_all | solution.py:11
  20.7 7.5 %all-to-all-done = bf16[16,16,256]{2,1,0:T(8,128)(2,1)S(1)} async-done(((bf16[16,16,256]{2,1,0:T(8,128)(2,1)}), bf16[16,16,256]{2,1,0:T(8,128)(2,1)S(1)}, u32[]{:S(2)}, u32[]{:S(2)}) %all-to-all-start) | async-done | bytes 131104 | tf_op jit(solution)/shard_map/all_to_all | solution.py:11
  31.6 11.6 %all_to_all.25 = bf16[16,16,256]{2,1,0:T(8,128)(2,1)S(1)} all-to-all(bf16[16,16,256]{2,1,0:T(8,128)(2,1)S(1)} %bitcast.105), channel_id=1, replica_groups=mesh['kv'=16,'tp'=16] {'tp'}, dimensions={0} | all-to-all | bytes 262144 | tf_op jit(solution)/shard_map/all_to_all | solution.py:35
  43.8 11.6 %all_to_all.26 = bf16[16,16,256]{2,1,0:T(8,128)(2,1)S(1)} all-to-all(bf16[16,16,256]{2,1,0:T(8,128)(2,1)S(1)} %broadcast_in_dim.10), channel_id=1, replica_groups=mesh['kv'=16,'tp'=16] {'tp'}, dimensions={0} | all-to-all | bytes 262144 | tf_op jit(solution)/shard_map/all_to_all | solution.py:11
  55.7 1.6 broadcast_in_dim.11
  57.3 6.9 %all-to-all-start.3 = ((bf16[16,16,4096]{2,1,0:T(8,128)(2,1)}), bf16[16,16,4096]{2,1,0:T(8,128)(2,1)S(1)}, u32[]{:S(2)}, u32[]{:S(2)}) async-start(bf16[16,16,4096]{2,1,0:T(8,128)(2,1)} %broadcast_in_dim.11), calls=%async_computation.3 | async-start | bytes 4194304 | tf_op jit(solution)/shard_map/all_to_all | solution.py:11
  64.3 43.2 %all-to-all-done.3 = bf16[16,16,4096]{2,1,0:T(8,128)(2,1)S(1)} async-done(((bf16[16,16,4096]{2,1,0:T(8,128)(2,1)}), bf16[16,16,4096]{2,1,0:T(8,128)(2,1)S(1)}, u32[]{:S(2)}, u32[]{:S(2)}) %all-to-all-start.3) | async-done | bytes 2097184 | tf_op jit(solution)/shard_map/all_to_all | solution.py:11
  109.5 1.4 collective-permute-start.8
  110.9 2.2 %collective-permute-start.7 = (bf16[16,44]{0,1:T(8,128)(2,1)S(1)}, bf16[16,44]{0,1:T(8,128)(2,1)S(1)}, u32[]{:S(2)}, u32[]{:S(2)}) collective-permute-start(bf16[16,44]{0,1:T(8,128)(2,1)S(1)} %get-tuple-element.9), channel_id=1, source_target_pairs={{0,128},{16,144},{32,160},{48,176},{64,192},{80,208},{96,224},{112... | collective-permute-start | bytes 4232 | tf_op jit(solution)/shard_map/ppermute | solution.py:131
  113.2 3.2 %collective-permute-start.6 = (bf16[16,44]{0,1:T(8,128)(2,1)S(1)}, bf16[16,44]{0,1:T(8,128)(2,1)S(1)}, u32[]{:S(2)}, u32[]{:S(2)}) collective-permute-start(bf16[16,44]{0,1:T(8,128)(2,1)S(1)} %get-tuple-element.10), channel_id=1, source_target_pairs={{0,112},{16,96},{32,80},{48,64},{64,48},{80,32},{96,16},{112,0},{1... | collective-permute-start | bytes 4232 | tf_op jit(solution)/shard_map/ppermute | solution.py:131
  116.4 1.1 collective-permute-start.5
  117.7 0.8 collective-permute-start.3
  118.5 2.6 %collective-permute-start.2 = (bf16[16,44]{0,1:T(8,128)(2,1)S(1)}, bf16[16,44]{0,1:T(8,128)(2,1)S(1)}, u32[]{:S(2)}, u32[]{:S(2)}) collective-permute-start(bf16[16,44]{0,1:T(8,128)(2,1)S(1)} %get-tuple-element.14), channel_id=1, source_target_pairs={{0,48},{16,32},{32,16},{48,0},{64,112},{80,96},{96,80},{112,64},{1... | collective-permute-start | bytes 4232 | tf_op jit(solution)/shard_map/ppermute | solution.py:131
  121.1 1.5 collective-permute-start.1
  122.6 2.4 %collective-permute-start.12 = (bf16[16,44]{0,1:T(8,128)(2,1)S(1)}, bf16[16,44]{0,1:T(8,128)(2,1)S(1)}, u32[]{:S(2)}, u32[]{:S(2)}) collective-permute-start(bf16[16,44]{0,1:T(8,128)(2,1)S(1)} %get-tuple-element.4), channel_id=1, source_target_pairs={{0,208},{16,192},{32,240},{48,224},{64,144},{80,128},{96,176},{112... | collective-permute-start | bytes 4232 | tf_op jit(solution)/shard_map/ppermute | solution.py:131
  125.0 2.9 %collective-permute-start.10 = (bf16[16,44]{0,1:T(8,128)(2,1)S(1)}, bf16[16,44]{0,1:T(8,128)(2,1)S(1)}, u32[]{:S(2)}, u32[]{:S(2)}) collective-permute-start(bf16[16,44]{0,1:T(8,128)(2,1)S(1)} %get-tuple-element.6), channel_id=1, source_target_pairs={{0,176},{16,160},{32,144},{48,128},{64,240},{80,224},{96,208},{112... | collective-permute-start | bytes 4232 | tf_op jit(solution)/shard_map/ppermute | solution.py:131
  127.8 1.8 %collective-permute-start.11 = (bf16[16,44]{0,1:T(8,128)(2,1)S(1)}, bf16[16,44]{0,1:T(8,128)(2,1)S(1)}, u32[]{:S(2)}, u32[]{:S(2)}) collective-permute-start(bf16[16,44]{0,1:T(8,128)(2,1)S(1)} %get-tuple-element.5), channel_id=1, source_target_pairs={{0,192},{16,208},{32,224},{48,240},{64,128},{80,144},{96,160},{112... | collective-permute-start | bytes 4232 | tf_op jit(solution)/shard_map/ppermute | solution.py:131
  130.2 3.5 %collective-permute-start.14 = (bf16[16,44]{0,1:T(8,128)(2,1)S(1)}, bf16[16,44]{0,1:T(8,128)(2,1)S(1)}, u32[]{:S(2)}, u32[]{:S(2)}) collective-permute-start(bf16[16,44]{0,1:T(8,128)(2,1)S(1)} %get-tuple-element.2), channel_id=1, source_target_pairs={{0,240},{16,224},{32,208},{48,192},{64,176},{80,160},{96,144},{112... | collective-permute-start | bytes 4232 | tf_op jit(solution)/shard_map/ppermute | solution.py:131
  137.6 8.0 %reshape.257 = bf16[704,4096]{1,0:T(8,128)(2,1)} reshape(bf16[16,44,4096]{2,1,0:T(8,128)(2,1)} %all-gather.3.cloned.1.call-done) | data formatting | bytes 11534336
  145.6 3.6 %fusion.31 = f32[16,4096]{1,0:T(8,128)S(1)} fusion(bf16[16,704]{0,1:T(8,128)(2,1)S(1)} %dynamic_update_slice.63, bf16[704,4096]{1,0:T(8,128)(2,1)} %reshape.257), kind=kOutput, calls=%fused_computation.76 | convolution fusion | flops 92274688 | bytes 6051840 | tf_op jit(solution)/shard_map/dot_general | solution.py:58
  149.9 10.2 %all-to-all-start.4 = ((f32[16,16,256]{2,1,0:T(8,128)}), f32[16,16,256]{2,1,0:T(8,128)S(1)}, u32[]{:S(2)}, u32[]{:S(2)}) async-start(f32[16,16,256]{2,1,0:T(8,128)} %bitcast.96), calls=%async_computation.4 | async-start | bytes 524288 | tf_op jit(solution)/shard_map/all_to_all | solution.py:41
  160.1 1.3 multiply_add_fusion
  161.5 10.2 %all-to-all-done.4 = f32[16,16,256]{2,1,0:T(8,128)S(1)} async-done(((f32[16,16,256]{2,1,0:T(8,128)}), f32[16,16,256]{2,1,0:T(8,128)S(1)}, u32[]{:S(2)}, u32[]{:S(2)}) %all-to-all-start.4) | async-done | bytes 262176 | tf_op jit(solution)/shard_map/all_to_all | solution.py:41
  (113 shorter events, 13.5 us)
Async XLA Ops:
  7.2 23.8 %copy-start = (bf16[128,4096]{1,0:T(8,128)(2,1)S(1)}, bf16[128,4096]{1,0:T(8,128)(2,1)}, u32[]{:S(2)}) copy-start(bf16[128,4096]{1,0:T(8,128)(2,1)} %param.24) | copy-start | bytes 3145732
  7.2 21.8 %copy-start.4 = (bf16[4096,128]{1,0:T(8,128)(2,1)S(1)}, bf16[4096,128]{1,0:T(8,128)(2,1)}, u32[]{:S(2)}) copy-start(bf16[4096,128]{1,0:T(8,128)(2,1)} %param.17) | copy-start | bytes 3145732
  7.2 130.3 %all-gather.3.cloned.1.call-start = ((), (), s32[]{:S(2)}) async-start(), calls=%async_computation.5 | async-start | bytes 6684672 | tf_op jit(solution)/shard_map/all_gather | solution.py:134
  9.3 18.9 %all-to-all-start = ((bf16[16,16,256]{2,1,0:T(8,128)(2,1)}), bf16[16,16,256]{2,1,0:T(8,128)(2,1)S(1)}, u32[]{:S(2)}, u32[]{:S(2)}) async-start(bf16[16,16,256]{2,1,0:T(8,128)(2,1)} %broadcast_in_dim.8), calls=%async_computation | async-start | bytes 262144 | tf_op jit(solution)/shard_map/all_to_all | solution.py:11
  31.0 24.5 %copy-start.13 = (f32[4096]{0:T(1024)S(1)}, f32[4096]{0:T(1024)}, u32[]{:S(2)}) copy-start(f32[4096]{0:T(1024)} %param.26) | copy-start | bytes 49156
  57.3 50.2 %copy-start.7 = (bf16[4096,44]{0,1:T(8,128)(2,1)S(1)}, bf16[4096,44]{0,1:T(8,128)(2,1)}, u32[]{:S(2)}) copy-start(bf16[4096,44]{0,1:T(8,128)(2,1)} %param.27) | copy-start | bytes 1081348
  57.3 50.2 %all-to-all-start.3 = ((bf16[16,16,4096]{2,1,0:T(8,128)(2,1)}), bf16[16,16,4096]{2,1,0:T(8,128)(2,1)S(1)}, u32[]{:S(2)}, u32[]{:S(2)}) async-start(bf16[16,16,4096]{2,1,0:T(8,128)(2,1)} %broadcast_in_dim.11), calls=%async_computation.3 | async-start | bytes 4194304 | tf_op jit(solution)/shard_map/all_to_all | solution.py:11
  109.4 8.0 %collective-permute-start.9 = (bf16[16,44]{0,1:T(8,128)(2,1)S(1)}, bf16[16,44]{0,1:T(8,128)(2,1)S(1)}, u32[]{:S(2)}, u32[]{:S(2)}) collective-permute-start(bf16[16,44]{0,1:T(8,128)(2,1)S(1)} %get-tuple-element.7), channel_id=1, source_target_pairs={{0,160},{16,176},{32,128},{48,144},{64,224},{80,240},{96,192},{112... | collective-permute-start | bytes 4232 | tf_op jit(solution)/shard_map/ppermute | solution.py:131
  109.5 8.1 %collective-permute-start.8 = (bf16[16,44]{0,1:T(8,128)(2,1)S(1)}, bf16[16,44]{0,1:T(8,128)(2,1)S(1)}, u32[]{:S(2)}, u32[]{:S(2)}) collective-permute-start(bf16[16,44]{0,1:T(8,128)(2,1)S(1)} %get-tuple-element.8), channel_id=1, source_target_pairs={{0,144},{16,128},{32,176},{48,160},{64,208},{80,192},{96,240},{112... | collective-permute-start | bytes 4232 | tf_op jit(solution)/shard_map/ppermute | solution.py:131
  110.9 7.6 %collective-permute-start.7 = (bf16[16,44]{0,1:T(8,128)(2,1)S(1)}, bf16[16,44]{0,1:T(8,128)(2,1)S(1)}, u32[]{:S(2)}, u32[]{:S(2)}) collective-permute-start(bf16[16,44]{0,1:T(8,128)(2,1)S(1)} %get-tuple-element.9), channel_id=1, source_target_pairs={{0,128},{16,144},{32,160},{48,176},{64,192},{80,208},{96,224},{112... | collective-permute-start | bytes 4232 | tf_op jit(solution)/shard_map/ppermute | solution.py:131
  113.2 7.9 %collective-permute-start.6 = (bf16[16,44]{0,1:T(8,128)(2,1)S(1)}, bf16[16,44]{0,1:T(8,128)(2,1)S(1)}, u32[]{:S(2)}, u32[]{:S(2)}) collective-permute-start(bf16[16,44]{0,1:T(8,128)(2,1)S(1)} %get-tuple-element.10), channel_id=1, source_target_pairs={{0,112},{16,96},{32,80},{48,64},{64,48},{80,32},{96,16},{112,0},{1... | collective-permute-start | bytes 4232 | tf_op jit(solution)/shard_map/ppermute | solution.py:131
  116.4 6.2 %collective-permute-start.5 = (bf16[16,44]{0,1:T(8,128)(2,1)S(1)}, bf16[16,44]{0,1:T(8,128)(2,1)S(1)}, u32[]{:S(2)}, u32[]{:S(2)}) collective-permute-start(bf16[16,44]{0,1:T(8,128)(2,1)S(1)} %get-tuple-element.11), channel_id=1, source_target_pairs={{0,96},{16,112},{32,64},{48,80},{64,32},{80,48},{96,0},{112,16},{1... | collective-permute-start | bytes 4232 | tf_op jit(solution)/shard_map/ppermute | solution.py:131
  117.4 5.1 %collective-permute-start.4 = (bf16[16,44]{0,1:T(8,128)(2,1)S(1)}, bf16[16,44]{0,1:T(8,128)(2,1)S(1)}, u32[]{:S(2)}, u32[]{:S(2)}) collective-permute-start(bf16[16,44]{0,1:T(8,128)(2,1)S(1)} %get-tuple-element.12), channel_id=1, source_target_pairs={{0,80},{16,64},{32,112},{48,96},{64,16},{80,0},{96,48},{112,32},{1... | collective-permute-start | bytes 4232 | tf_op jit(solution)/shard_map/ppermute | solution.py:131
  117.7 7.3 %collective-permute-start.3 = (bf16[16,44]{0,1:T(8,128)(2,1)S(1)}, bf16[16,44]{0,1:T(8,128)(2,1)S(1)}, u32[]{:S(2)}, u32[]{:S(2)}) collective-permute-start(bf16[16,44]{0,1:T(8,128)(2,1)S(1)} %get-tuple-element.13), channel_id=1, source_target_pairs={{0,64},{16,80},{32,96},{48,112},{64,0},{80,16},{96,32},{112,48},{1... | collective-permute-start | bytes 4232 | tf_op jit(solution)/shard_map/ppermute | solution.py:131
  118.5 9.3 %collective-permute-start.2 = (bf16[16,44]{0,1:T(8,128)(2,1)S(1)}, bf16[16,44]{0,1:T(8,128)(2,1)S(1)}, u32[]{:S(2)}, u32[]{:S(2)}) collective-permute-start(bf16[16,44]{0,1:T(8,128)(2,1)S(1)} %get-tuple-element.14), channel_id=1, source_target_pairs={{0,48},{16,32},{32,16},{48,0},{64,112},{80,96},{96,80},{112,64},{1... | collective-permute-start | bytes 4232 | tf_op jit(solution)/shard_map/ppermute | solution.py:131
  121.1 8.6 %collective-permute-start.1 = (bf16[16,44]{0,1:T(8,128)(2,1)S(1)}, bf16[16,44]{0,1:T(8,128)(2,1)S(1)}, u32[]{:S(2)}, u32[]{:S(2)}) collective-permute-start(bf16[16,44]{0,1:T(8,128)(2,1)S(1)} %get-tuple-element.15), channel_id=1, source_target_pairs={{0,32},{16,48},{32,0},{48,16},{64,96},{80,112},{96,64},{112,80},{1... | collective-permute-start | bytes 4232 | tf_op jit(solution)/shard_map/ppermute | solution.py:131
  122.6 7.6 %collective-permute-start = (bf16[16,44]{0,1:T(8,128)(2,1)S(1)}, bf16[16,44]{0,1:T(8,128)(2,1)S(1)}, u32[]{:S(2)}, u32[]{:S(2)}) collective-permute-start(bf16[16,44]{0,1:T(8,128)(2,1)S(1)} %get-tuple-element.16), channel_id=1, source_target_pairs={{0,16},{16,0},{32,48},{48,32},{64,80},{80,64},{96,112},{112,96},{1... | collective-permute-start | bytes 4232 | tf_op jit(solution)/shard_map/ppermute | solution.py:131
  122.6 14.2 %collective-permute-start.12 = (bf16[16,44]{0,1:T(8,128)(2,1)S(1)}, bf16[16,44]{0,1:T(8,128)(2,1)S(1)}, u32[]{:S(2)}, u32[]{:S(2)}) collective-permute-start(bf16[16,44]{0,1:T(8,128)(2,1)S(1)} %get-tuple-element.4), channel_id=1, source_target_pairs={{0,208},{16,192},{32,240},{48,224},{64,144},{80,128},{96,176},{112... | collective-permute-start | bytes 4232 | tf_op jit(solution)/shard_map/ppermute | solution.py:131
  125.0 11.3 %collective-permute-start.10 = (bf16[16,44]{0,1:T(8,128)(2,1)S(1)}, bf16[16,44]{0,1:T(8,128)(2,1)S(1)}, u32[]{:S(2)}, u32[]{:S(2)}) collective-permute-start(bf16[16,44]{0,1:T(8,128)(2,1)S(1)} %get-tuple-element.6), channel_id=1, source_target_pairs={{0,176},{16,160},{32,144},{48,128},{64,240},{80,224},{96,208},{112... | collective-permute-start | bytes 4232 | tf_op jit(solution)/shard_map/ppermute | solution.py:131
  127.8 8.7 %collective-permute-start.11 = (bf16[16,44]{0,1:T(8,128)(2,1)S(1)}, bf16[16,44]{0,1:T(8,128)(2,1)S(1)}, u32[]{:S(2)}, u32[]{:S(2)}) collective-permute-start(bf16[16,44]{0,1:T(8,128)(2,1)S(1)} %get-tuple-element.5), channel_id=1, source_target_pairs={{0,192},{16,208},{32,224},{48,240},{64,128},{80,144},{96,160},{112... | collective-permute-start | bytes 4232 | tf_op jit(solution)/shard_map/ppermute | solution.py:131
  129.6 7.4 %collective-permute-start.13 = (bf16[16,44]{0,1:T(8,128)(2,1)S(1)}, bf16[16,44]{0,1:T(8,128)(2,1)S(1)}, u32[]{:S(2)}, u32[]{:S(2)}) collective-permute-start(bf16[16,44]{0,1:T(8,128)(2,1)S(1)} %get-tuple-element.3), channel_id=1, source_target_pairs={{0,224},{16,240},{32,192},{48,208},{64,160},{80,176},{96,128},{112... | collective-permute-start | bytes 4232 | tf_op jit(solution)/shard_map/ppermute | solution.py:131
  130.2 7.2 %collective-permute-start.14 = (bf16[16,44]{0,1:T(8,128)(2,1)S(1)}, bf16[16,44]{0,1:T(8,128)(2,1)S(1)}, u32[]{:S(2)}, u32[]{:S(2)}) collective-permute-start(bf16[16,44]{0,1:T(8,128)(2,1)S(1)} %get-tuple-element.2), channel_id=1, source_target_pairs={{0,240},{16,224},{32,208},{48,192},{64,176},{80,160},{96,144},{112... | collective-permute-start | bytes 4232 | tf_op jit(solution)/shard_map/ppermute | solution.py:131
  149.2 22.5 %copy-start.10 = (bf16[16,256]{1,0:T(8,128)(2,1)S(1)}, bf16[16,256]{1,0:T(8,128)(2,1)}, u32[]{:S(2)}) copy-start(bf16[16,256]{1,0:T(8,128)(2,1)} %copy-done.9) | copy-start | bytes 24580
  149.9 21.8 %all-to-all-start.4 = ((f32[16,16,256]{2,1,0:T(8,128)}), f32[16,16,256]{2,1,0:T(8,128)S(1)}, u32[]{:S(2)}, u32[]{:S(2)}) async-start(f32[16,16,256]{2,1,0:T(8,128)} %bitcast.96), calls=%async_computation.4 | async-start | bytes 524288 | tf_op jit(solution)/shard_map/all_to_all | solution.py:41
  (13 other events, 95.7 us)
Sparse Core Ops, SparseCore 0:
  10.4 91.0 all-gather.2
